TPU v7x, 32 devices: a whole 2x2x4 slice. The times are simulated.
32 devices in a mesh: fs: 8 (over z, core), tp: 4 (over y, x).
Axes of the slice: x: 2, y: 2, z: 4, core: 2. Of those that a mesh axis runs over, the one named last changes fastest.
Arguments:
- tokens: bfloat16 [4096, 4096], P('fs', 'tp'), may hold values from -16 to 16
- norm_gain: float32 [4096], P('fs'), may hold values from 0.1 to 1.9
- gate_train: float32 [4096, 12288], P('fs', 'tp'), may hold values from -6 to 6
- up_train: float32 [4096, 12288], P('fs', 'tp'), may hold values from -6 to 6
Outputs:
- gate_serve: bfloat16 [4096, 12288], P(None, 'tp')
- up_serve: bfloat16 [4096, 12288], P(None, 'tp')
- hidden: bfloat16 [4096, 12288], P('fs', 'tp')
All inputs are finite; a program needn't handle non-finite values.
Results may differ from a plain program's by a relative error of at most 0.0071.
Values may be sent and summed in bfloat16 or wider, within the bound.
A program may use at most 192 MiB of HBM per device.

v0:
```python
import jax
import jax.numpy as jnp
from jax import lax
from jax.sharding import PartitionSpec as P


def body(tokens, norm_gain, gate_train, up_train):
    gain = norm_gain[:, None]
    gate_local = (gate_train * gain).astype(jnp.bfloat16)
    up_local = (up_train * gain).astype(jnp.bfloat16)
    whole = lax.all_gather(tokens, "tp", axis=1, tiled=True)
    values = whole.astype(jnp.float32)
    normed = (values * lax.rsqrt(jnp.mean(values * values, axis=-1, keepdims=True) + 1e-06)).astype(
        jnp.bfloat16
    )
    width = normed.shape[1]
    scale = width ** (-0.5)
    gate_serve, up_serve = (
        lax.all_gather(gate_local, "fs", axis=0, tiled=True),
        lax.all_gather(up_local, "fs", axis=0, tiled=True),
    )
    gate_acc = jnp.dot(normed, gate_serve, preferred_element_type=jnp.float32)
    up_acc = jnp.dot(normed, up_serve, preferred_element_type=jnp.float32)
    gate = gate_acc * scale
    up = up_acc * scale
    hidden = (jax.nn.silu(gate) * up).astype(jnp.bfloat16)
    return (gate_serve, up_serve, hidden)


def solution(mesh):
    in_specs = (P("fs", "tp"), P("fs"), P("fs", "tp"), P("fs", "tp"))
    out_specs = (P(None, "tp"), P(None, "tp"), P("fs", "tp"))
    return jax.shard_map(body, mesh=mesh, in_specs=in_specs, out_specs=out_specs, check_vma=False)
```

profile of v0, /device:TPU:0, one launch (start us, length us, event | category | flops | bytes accessed | tf_op | source)
XLA Modules:
  0.0 569.7 jit_solution(12411793271498854987)
XLA Ops:
  7.2 0.0 all-gather.8.cloned.1.call-start
  7.2 0.7 all-gather.8.cloned.1.call-update
  7.9 0.0 all-gather.4.cloned.1.call-start
  7.9 9.3 %multiply_convert_fusion.1 = (bf16[512,3072]{1,0:T(8,128)(2,1)}, bf16[512,3072]{1,0:T(8,128)(2,1)}) fusion(f32[512,3072]{1,0:T(8,128)} %param.7, f32[512]{0:T(512)} %param.5, f32[512,3072]{1,0:T(8,128)} %param.6), kind=kLoop, calls=%fused_computation.5 | loop fusion | flops 6291456 | bytes 18876416 | tf_op jit(solution)/shard_map/convert_element_type | solution.py:10
  17.2 0.0 all-gather.4.cloned.1.call-update
  17.3 0.0 all-gather.6.cloned.1.call-start
  17.3 0.7 all-gather.6.cloned.1.call-update
  18.0 47.2 %all-gather.8.cloned.1.call-done = bf16[512,4096]{1,0:T(8,128)(2,1)} async-done(((bf16[512,1024]{1,0:T(8,128)(2,1)}), bf16[512,4096]{1,0:T(8,128)(2,1)}) %all-gather.8.cloned.1.call-update) | async-done | bytes 4194320 | tf_op jit(solution)/shard_map/all_gather | solution.py:11
  65.1 3.1 fusion
  68.2 219.0 %all-gather.4.cloned.1.call-done = bf16[4096,3072]{1,0:T(8,128)(2,1)} async-done(((bf16[512,3072]{1,0:T(8,128)(2,1)}), bf16[4096,3072]{1,0:T(8,128)(2,1)}) %all-gather.4.cloned.1.call-update) | async-done | bytes 25165840 | tf_op jit(solution)/shard_map/all_gather | solution.py:19
  287.2 20.6 %fusion.3 = f32[512,3072]{1,0:T(8,128)} fusion(bf16[4096,3072]{1,0:T(8,128)(2,1)} %all-gather.4.cloned.1.call-done, bf16[512,4096]{1,0:T(8,128)(2,1)} %all-gather.8.cloned.1.call-done, f32[512]{0:T(512)S(1)} %add_rsqrt_fusion), kind=kOutput, calls=%fused_computation.7 | convolution fusion | flops 12891193344 | bytes 35653632 | tf_op jit(solution)/shard_map/dot_general | solution.py:22
  307.8 199.7 %all-gather.6.cloned.1.call-done = bf16[4096,3072]{1,0:T(8,128)(2,1)} async-done(((bf16[512,3072]{1,0:T(8,128)(2,1)}), bf16[4096,3072]{1,0:T(8,128)(2,1)}) %all-gather.6.cloned.1.call-update) | async-done | bytes 25165840 | tf_op jit(solution)/shard_map/all_gather | solution.py:20
  507.5 21.8 %multiply_convert_fusion = bf16[512,3072]{1,0:T(8,128)(2,1)} fusion(f32[512,3072]{1,0:T(8,128)} %fusion.3, bf16[4096,3072]{1,0:T(8,128)(2,1)} %all-gather.6.cloned.1.call-done, bf16[512,4096]{1,0:T(8,128)(2,1)} %all-gather.8.cloned.1.call-done, f32[512]{0:T(512)S(1)} %add_rsqrt_fusion), kind=kOutput, calls=%fused_computation.4 | convolution fusion | flops 12903776256 | bytes 38799360 | tf_op jit(solution)/shard_map/dot_general | solution.py:23
  529.4 0.0 copy-start
  529.4 22.0 %copy.9 = bf16[4096,3072]{1,0:T(8,128)(2,1)} copy(bf16[4096,3072]{1,0:T(8,128)(2,1)} %all-gather.4.cloned.1.call-done) | data formatting | bytes 50331648
  551.3 2.9 copy-done
  554.3 8.9 %copy.10 = bf16[4096,3072]{1,0:T(8,128)(2,1)} copy(bf16[4096,3072]{1,0:T(8,128)(2,1)S(1)} %copy-done) | data formatting | bytes 50331648
  (1 shorter events, 0.0 us)
Async XLA Ops:
  7.2 58.0 %all-gather.8.cloned.1.call-start = ((), (), s32[]{:S(2)}) async-start(), calls=%async_computation.2 | async-start | bytes 5242880 | tf_op jit(solution)/shard_map/all_gather | solution.py:11
  7.9 279.3 %all-gather.4.cloned.1.call-start = ((), (), s32[]{:S(2)}) async-start(), calls=%async_computation | async-start | bytes 28311552 | tf_op jit(solution)/shard_map/all_gather | solution.py:19
  17.3 490.3 %all-gather.6.cloned.1.call-start = ((), (), s32[]{:S(2)}) async-start(), calls=%async_computation.1 | async-start | bytes 28311552 | tf_op jit(solution)/shard_map/all_gather | solution.py:20
  529.4 24.9 %copy-start = (bf16[4096,3072]{1,0:T(8,128)(2,1)S(1)}, bf16[4096,3072]{1,0:T(8,128)(2,1)}, u32[]{:S(2)}) copy-start(bf16[4096,3072]{1,0:T(8,128)(2,1)} %all-gather.6.cloned.1.call-done) | copy-start | bytes 75497472
Sparse Core Ops, SparseCore 0:
  9.8 55.2 all-gather.7
  67.4 219.8 all-gather.3
  289.5 218.0 all-gather.5
where the time goes:
time: 570 us
  waiting for transfers between devices  467 us (82%)
  matrix products  42.4 us (7%)
  local copies, waits for them, and re-layouts  33.8 us (6%)
  between operations  13.7 us (2%)
  other arithmetic  12.4 us (2%)
    all_gather x1, waiting for transfers between devices, body(): lax.all_gather(gate_local, 'fs', axis=0, tiled=True)  219 us
    all_gather x1, waiting for transfers between devices, body(): lax.all_gather(up_local, 'fs', axis=0, tiled=True)  200 us
    all_gather x1, waiting for transfers between devices, body(): whole = lax.all_gather(tokens, 'tp', axis=1, tiled=True)  47.2 us
    unnamed x4, local copies, waits for them, and re-layouts  33.8 us
    dot_general x1, matrix products, body(): up_acc = jnp.dot(normed, up_serve, preferred_element_type=jnp.float32)  21.8 us
    dot_general x1, matrix products, body(): gate_acc = jnp.dot(normed, gate_serve, preferred_element_type=jnp.float32)  20.6 us
  transfers between devices with their start and end apart: 3, of which 3 were waited for; matrix products, arithmetic and copies ran while one was open for 6% of the time, Pallas kernels for 0%

commit v1 on v0

--- a/solution.py
+++ b/solution.py
@@ -8,7 +8,12 @@
     gain = norm_gain[:, None]
     gate_local = (gate_train * gain).astype(jnp.bfloat16)
     up_local = (up_train * gain).astype(jnp.bfloat16)
-    whole = lax.all_gather(tokens, "tp", axis=1, tiled=True)
+    ring = [tokens]
+    for hop in range(3):
+        ring.append(lax.ppermute(ring[-1], "tp", [(dev, (dev + 1) % 4) for dev in range(4)]))
+    whole = jnp.roll(
+        jnp.concatenate(ring[::-1], axis=1), (lax.axis_index("tp") + 1) * ring[0].shape[1], axis=1
+    )
     values = whole.astype(jnp.float32)
     normed = (values * lax.rsqrt(jnp.mean(values * values, axis=-1, keepdims=True) + 1e-06)).astype(
         jnp.bfloat16

time: 570 us -> 522 us (0.916)
  waiting for transfers between devices: 467 us -> 411 us
  local copies, waits for them, and re-layouts: 33.8 us -> 40.4 us
    all_gather x1, waiting for transfers between devices: 219 us -> 137 us  [body(): lax.all_gather(gate_local, 'fs', axis=0, tiled=True)]
    ppermute x0 -> x3, waiting for transfers between devices: none -> 73.3 us  [body(): lax.ppermute(ring[-1], 'tp', [(dev, (dev + 1) % 4) for dev in range(4)])]
    all_gather x1 -> x0, waiting for transfers between devices: 47.2 us -> none  [body(): whole = lax.all_gather(tokens, 'tp', axis=1, tiled=True)]
    unnamed x4 -> x15, local copies, waits for them, and re-layouts: 33.8 us -> 40.3 us
  transfers between devices with their start and end apart: 3 -> 5, of which waited for: 3 -> 5; matrix products, arithmetic and copies ran while one was open for 6% -> 5% of each run, Pallas kernels for 0% -> 0%
where the time goes in v1:
time: 522 us
  waiting for transfers between devices  411 us (79%)
  matrix products  42.5 us (8%)
  local copies, waits for them, and re-layouts  40.4 us (8%)
  between operations  14.1 us (3%)
  other arithmetic  10.3 us (2%)
    all_gather x1, waiting for transfers between devices, body(): lax.all_gather(up_local, 'fs', axis=0, tiled=True)  200 us
    all_gather x1, waiting for transfers between devices, body(): lax.all_gather(gate_local, 'fs', axis=0, tiled=True)  137 us
    ppermute x3, waiting for transfers between devices, body(): lax.ppermute(ring[-1], 'tp', [(dev, (dev + 1) % 4) for dev in range(4)])  73.3 us
    unnamed x15, local copies, waits for them, and re-layouts  40.3 us
    dot_general x1, matrix products, body(): up_acc = jnp.dot(normed, up_serve, preferred_element_type=jnp.float32)  22 us
    dot_general x1, matrix products, body(): gate_acc = jnp.dot(normed, gate_serve, preferred_element_type=jnp.float32)  20.5 us
  transfers between devices with their start and end apart: 5, of which 5 were waited for; matrix products, arithmetic and copies ran while one was open for 5% of the time, Pallas kernels for 0%

profile of v1, /device:TPU:0, one launch (start us, length us, event | category | flops | bytes accessed | tf_op | source)
XLA Modules:
  0.0 522.2 jit_solution(16411072097817935836)
XLA Ops:
  7.2 9.4 %multiply_convert_fusion.1 = (bf16[512,3072]{1,0:T(8,128)(2,1)}, bf16[512,3072]{1,0:T(8,128)(2,1)}) fusion(f32[512,3072]{1,0:T(8,128)} %param.7, f32[512]{0:T(512)} %param.5, f32[512,3072]{1,0:T(8,128)} %param.6), kind=kLoop, calls=%fused_computation.5 | loop fusion | flops 6291456 | bytes 18876416 | tf_op jit(solution)/shard_map/convert_element_type | solution.py:10
  16.7 0.7 all-gather.5.cloned.1.call-update
  17.4 3.0 collective-permute-start
  20.4 24.1 %collective-permute-done = bf16[512,1024]{1,0:T(8,128)(2,1)S(1)} collective-permute-done((bf16[512,1024]{1,0:T(8,128)(2,1)S(1)}, bf16[512,1024]{1,0:T(8,128)(2,1)S(1)}, u32[]{:S(2)}, u32[]{:S(2)}) %collective-permute-start) | collective-permute-done | bytes 1048608 | tf_op jit(solution)/shard_map/ppermute | solution.py:13
  44.5 0.8 collective-permute-start.1
  45.3 24.5 %collective-permute-done.1 = bf16[512,1024]{1,0:T(8,128)(2,1)S(1)} collective-permute-done((bf16[512,1024]{1,0:T(8,128)(2,1)S(1)}, bf16[512,1024]{1,0:T(8,128)(2,1)S(1)}, u32[]{:S(2)}, u32[]{:S(2)}) %collective-permute-start.1) | collective-permute-done | bytes 1048608 | tf_op jit(solution)/shard_map/ppermute | solution.py:13
  69.8 24.7 %collective-permute-done.2 = bf16[512,1024]{1,0:T(8,128)(2,1)} collective-permute-done((bf16[512,1024]{1,0:T(8,128)(2,1)S(1)}, bf16[512,1024]{1,0:T(8,128)(2,1)}, u32[]{:S(2)}, u32[]{:S(2)}) %collective-permute-start.2) | collective-permute-done | bytes 1048608 | tf_op jit(solution)/shard_map/ppermute | solution.py:13
  94.5 1.3 constant_dynamic-update-slice_fusion.7
  95.8 0.1 constant_dynamic-update-slice_fusion.6
  95.9 0.1 constant_dynamic-update-slice_fusion.5
  96.0 0.1 constant_dynamic-update-slice_fusion.4
  96.1 1.3 constant_dynamic-update-slice_fusion.3
  97.5 0.1 constant_dynamic-update-slice_fusion.2
  97.6 0.1 constant_dynamic-update-slice_fusion.1
  97.6 0.1 constant_dynamic-update-slice_fusion
  97.8 3.4 copy-done.2
  101.1 0.9 fusion
  102.0 137.3 %all-gather.3.cloned.1.call-done = bf16[4096,3072]{1,0:T(8,128)(2,1)} async-done(((bf16[512,3072]{1,0:T(8,128)(2,1)}), bf16[4096,3072]{1,0:T(8,128)(2,1)}) %all-gather.3.cloned.1.call-update) | async-done | bytes 25165840 | tf_op jit(solution)/shard_map/all_gather | solution.py:24
  239.3 20.5 %fusion.3 = f32[512,3072]{1,0:T(8,128)} fusion(bf16[4096,3072]{1,0:T(8,128)(2,1)} %all-gather.3.cloned.1.call-done, f32[512]{0:T(512)S(1)} %add_rsqrt_fusion, bf16[512,8192]{1,0:T(8,128)(2,1)} %copy-done.2, s32[]{:T(128)S(6)} %select_n.14), kind=kOutput, calls=%fused_computation.7 | convolution fusion | flops 12891193344 | bytes 35653636 | tf_op jit(solution)/shard_map/dot_general | solution.py:27
  259.8 199.8 %all-gather.5.cloned.1.call-done = bf16[4096,3072]{1,0:T(8,128)(2,1)} async-done(((bf16[512,3072]{1,0:T(8,128)(2,1)}), bf16[4096,3072]{1,0:T(8,128)(2,1)}) %all-gather.5.cloned.1.call-update) | async-done | bytes 25165840 | tf_op jit(solution)/shard_map/all_gather | solution.py:25
  459.6 22.0 %multiply_convert_fusion = bf16[512,3072]{1,0:T(8,128)(2,1)} fusion(f32[512,3072]{1,0:T(8,128)} %fusion.3, bf16[4096,3072]{1,0:T(8,128)(2,1)} %all-gather.5.cloned.1.call-done, f32[512]{0:T(512)S(1)} %add_rsqrt_fusion, bf16[512,8192]{1,0:T(8,128)(2,1)} %copy-done.2, s32[]{:T(128)S(6)} %select_n.14), kind=kOutput, calls=%fused_computation.4 | convolution fusion | flops 12903776256 | bytes 38799364 | tf_op jit(solution)/shard_map/dot_general | solution.py:28
  481.6 22.0 %copy.16 = bf16[4096,3072]{1,0:T(8,128)(2,1)} copy(bf16[4096,3072]{1,0:T(8,128)(2,1)} %all-gather.3.cloned.1.call-done) | data formatting | bytes 50331648
  503.5 2.9 copy-done
  506.5 8.9 %copy.17 = bf16[4096,3072]{1,0:T(8,128)(2,1)} copy(bf16[4096,3072]{1,0:T(8,128)(2,1)S(1)} %copy-done) | data formatting | bytes 50331648
  (9 shorter events, 0.1 us)
Async XLA Ops:
  7.2 10.2 %copy-start.1 = (bf16[512,1024]{1,0:T(8,128)(2,1)S(1)}, bf16[512,1024]{1,0:T(8,128)(2,1)}, u32[]{:S(2)}) copy-start(bf16[512,1024]{1,0:T(8,128)(2,1)} %param.4) | copy-start | bytes 3145732
  7.2 232.2 %all-gather.3.cloned.1.call-start = ((), (), s32[]{:S(2)}) async-start(), calls=%async_computation | async-start | bytes 28311552 | tf_op jit(solution)/shard_map/all_gather | solution.py:24
  16.6 443.0 %all-gather.5.cloned.1.call-start = ((), (), s32[]{:S(2)}) async-start(), calls=%async_computation.1 | async-start | bytes 28311552 | tf_op jit(solution)/shard_map/all_gather | solution.py:25
  17.4 27.1 %collective-permute-start = (bf16[512,1024]{1,0:T(8,128)(2,1)S(1)}, bf16[512,1024]{1,0:T(8,128)(2,1)S(1)}, u32[]{:S(2)}, u32[]{:S(2)}) collective-permute-start(bf16[512,1024]{1,0:T(8,128)(2,1)S(1)} %copy-done.1), channel_id=1, source_target_pairs={{0,1},{1,2},{2,3},{3,0},{4,5},{5,6},{6,7},{7,4},{8,9},{9,10},{10,1... | collective-permute-start | bytes 3145736 | tf_op jit(solution)/shard_map/ppermute | solution.py:13
  44.5 25.3 %collective-permute-start.1 = (bf16[512,1024]{1,0:T(8,128)(2,1)S(1)}, bf16[512,1024]{1,0:T(8,128)(2,1)S(1)}, u32[]{:S(2)}, u32[]{:S(2)}) collective-permute-start(bf16[512,1024]{1,0:T(8,128)(2,1)S(1)} %collective-permute-done), channel_id=1, source_target_pairs={{0,1},{1,2},{2,3},{3,0},{4,5},{5,6},{6,7},{7,4},{8,9},{9,10},{10,1... | collective-permute-start | bytes 3145736 | tf_op jit(solution)/shard_map/ppermute | solution.py:13
  69.8 24.7 %collective-permute-start.2 = (bf16[512,1024]{1,0:T(8,128)(2,1)S(1)}, bf16[512,1024]{1,0:T(8,128)(2,1)}, u32[]{:S(2)}, u32[]{:S(2)}) collective-permute-start(bf16[512,1024]{1,0:T(8,128)(2,1)S(1)} %collective-permute-done.1), channel_id=1, source_target_pairs={{0,1},{1,2},{2,3},{3,0},{4,5},{5,6},{6,7},{7,4},{8,9},{9,10},{10,1... | collective-permute-start | bytes 3145736 | tf_op jit(solution)/shard_map/ppermute | solution.py:13
  97.7 3.4 copy-start.2
  481.6 24.9 %copy-start = (bf16[4096,3072]{1,0:T(8,128)(2,1)S(1)}, bf16[4096,3072]{1,0:T(8,128)(2,1)}, u32[]{:S(2)}) copy-start(bf16[4096,3072]{1,0:T(8,128)(2,1)} %all-gather.5.cloned.1.call-done) | copy-start | bytes 75497472
Sparse Core Ops, SparseCore 0:
  16.7 222.5 all-gather.2
  241.5 218.0 all-gather.4
